TPU v7x, 32 devices: a whole 2x2x4 slice. The times are simulated.
32 devices in a mesh: rep: 2 (over x), fs: 8 (over z, y), tp: 2 (over core).
Axes of the slice: x: 2, y: 2, z: 4, core: 2. Of those that a mesh axis runs over, the one named last changes fastest.
Arguments:
- tokens: bfloat16 [4096, 1024], P(('rep', 'fs', 'tp')), may hold values from -4 to 4
- mixer_out: bfloat16 [4096, 1024], P(('rep', 'fs')), may hold values from -4 to 4
- gain_first: float32 [1024], replicated, may hold values from 0.1 to 1.9
- gate_first: bfloat16 [1024, 2816], P('fs', 'tp'), may hold values from -0.1875 to 0.1875
- up_first: bfloat16 [1024, 2816], P('fs', 'tp'), may hold values from -0.1875 to 0.1875
- down_first: bfloat16 [2816, 1024], P('tp', 'fs'), may hold values from -0.109375 to 0.109375
- gain_second: float32 [1024], replicated, may hold values from 0.1 to 1.9
- gate_second: bfloat16 [1024, 2816], P('fs', 'tp'), may hold values from -0.1875 to 0.1875
- up_second: bfloat16 [1024, 2816], P('fs', 'tp'), may hold values from -0.1875 to 0.1875
- down_second: bfloat16 [2816, 1024], P('tp', 'fs'), may hold values from -0.109375 to 0.109375
- gain_last: float32 [1024], P('tp'), may hold values from 0.1 to 1.9
Outputs:
- result: bfloat16 [4096, 1024], P(('rep', 'fs'), 'tp')
All inputs are finite; a program needn't handle non-finite values.
Results may differ from a plain program's by a relative error of at most 0.02.
Values may be sent and summed in bfloat16 or wider, within the bound.
A program may use at most 64 MiB of HBM per device.

v0:
```python
import jax
import jax.numpy as jnp
from jax import lax
from jax.sharding import PartitionSpec as P

EPS = 1e-06


def over_all(slab, axis, dim):

    def gathered(part):
        return lax.all_gather(part, axis, axis=dim, tiled=True)

    return jax.tree.map(gathered, slab)


def normalize(floats_in, gain_vec):
    floats = floats_in.astype(jnp.float32)
    factor = lax.rsqrt(jnp.mean(floats * floats, axis=-1, keepdims=True) + EPS)
    return (floats * factor * gain_vec.astype(jnp.float32)).astype(jnp.bfloat16)


def gather_group(row_block):
    return lax.all_gather(row_block, "tp", axis=0, tiled=True)


def inner_hidden(normed, w_gate, w_up):

    def add_both(totals, pieces):
        columns = lax.slice_in_dim(normed, 0, pieces[0].shape[0], axis=1)
        return (
            totals[0] + jnp.dot(columns, pieces[0], preferred_element_type=jnp.float32),
            totals[1] + jnp.dot(columns, pieces[1], preferred_element_type=jnp.float32),
        )

    empty = jnp.zeros((normed.shape[0], w_gate.shape[1]), jnp.float32)
    gate_acc, up_acc = add_both((empty, empty), over_all((w_gate, w_up), "fs", 0))
    return (jax.nn.silu(gate_acc) * up_acc).astype(jnp.bfloat16)


def outer_weight(w_down):
    return lax.all_gather(w_down, "fs", axis=1, tiled=True)


def local(
    tokens,
    mixer_out,
    gain_first,
    gate_first,
    up_first,
    down_first,
    gain_second,
    gate_second,
    up_second,
    down_second,
    gain_last,
):
    rows_dev = tokens.shape[0]
    tp_count = lax.axis_size("tp")
    tp_index = lax.axis_index("tp")
    normed_own = normalize(tokens, gain_first)
    normed_one = gather_group(normed_own)
    hidden_one = inner_hidden(normed_one, gate_first, up_first)
    down_full = outer_weight(down_first)

    def row_terms():
        picked = lax.slice_in_dim(hidden_one, 0, rows_dev * lax.axis_size("tp"), axis=0)
        return jnp.dot(picked, down_full, preferred_element_type=jnp.float32)

    ffn_one = lax.psum_scatter(
        row_terms().astype(jnp.bfloat16), "tp", scatter_dimension=0, tiled=True
    ).astype(jnp.float32)
    after_one = (tokens.astype(jnp.float32) + 0.5 * ffn_one).astype(jnp.bfloat16)
    own_mixer = lax.dynamic_slice_in_dim(mixer_out, tp_index * rows_dev, rows_dev, 0)
    mixed_in = (after_one.astype(jnp.float32) + own_mixer.astype(jnp.float32)).astype(jnp.bfloat16)
    gathered = gather_group(mixed_in)
    normed_two = normalize(gathered, gain_second)
    hidden_two = inner_hidden(normed_two, gate_second, up_second)
    down_two_full = outer_weight(down_second)
    terms_two = jnp.dot(hidden_two, down_two_full, preferred_element_type=jnp.float32)
    ffn_two = lax.psum_scatter(
        terms_two.astype(jnp.bfloat16), "tp", scatter_dimension=1, tiled=True
    ).astype(jnp.float32)
    col_width = ffn_two.shape[1]
    my_cols = lax.dynamic_slice_in_dim(gathered, tp_index * col_width, col_width, 1)
    after_two = (my_cols.astype(jnp.float32) + 0.5 * ffn_two).astype(jnp.bfloat16)
    floats = after_two.astype(jnp.float32)
    sum_sq = lax.psum(jnp.sum(floats * floats, axis=1), "tp")
    factor = lax.rsqrt(sum_sq / (col_width * tp_count) + EPS)
    return (floats * factor[:, None] * gain_last.astype(jnp.float32)[None, :]).astype(jnp.bfloat16)


def solution(mesh):
    in_specs = (
        P(("rep", "fs", "tp"), None),
        P(("rep", "fs"), None),
        P(),
        P("fs", "tp"),
        P("fs", "tp"),
        P("tp", "fs"),
        P(),
        P("fs", "tp"),
        P("fs", "tp"),
        P("tp", "fs"),
        P("tp"),
    )
    out_specs = P(("rep", "fs"), "tp")
    return jax.shard_map(local, mesh=mesh, in_specs=in_specs, out_specs=out_specs, check_vma=False)
```

profile of v0, /device:TPU:0, one launch (start us, length us, event | category | flops | bytes accessed | tf_op | source)
XLA Modules:
  0.0 403.8 jit_solution(16282262251810732455)
XLA Ops:
  6.5 0.0 all-gather.7.cloned.1.call-start
  6.5 0.7 all-gather.7.cloned.1.call-update
  7.3 0.0 all-gather.11.cloned.1.call-start
  7.3 0.7 all-gather.11.cloned.1.call-update
  8.0 0.0 all-gather.9.cloned.1.call-start
  8.1 0.7 all-gather.9.cloned.1.call-update
  8.7 0.0 reduce-scatter.3.cloned.1.call-start
  8.8 1.1 fusion.10
  9.9 1.1 fusion.12
  11.0 2.3 all_gather.24
  13.3 56.1 %all-gather.7.cloned.1.call-done = bf16[1024,1408]{1,0:T(8,128)(2,1)} async-done(((bf16[128,1408]{1,0:T(8,128)(2,1)}), bf16[1024,1408]{1,0:T(8,128)(2,1)}) %all-gather.7.cloned.1.call-update) | async-done | bytes 2883600 | tf_op jit(solution)/shard_map/all_gather | solution.py:12
  69.4 2.8 fusion.20
  72.2 0.0 copy-start
  72.2 0.0 copy-start.1
  72.2 58.1 %all-gather.11.cloned.1.call-done = bf16[1408,1024]{1,0:T(8,128)(2,1)} async-done(((bf16[1408,128]{1,0:T(8,128)(2,1)}), bf16[1408,1024]{1,0:T(8,128)(2,1)}) %all-gather.11.cloned.1.call-update) | async-done | bytes 2883600 | tf_op jit(solution)/shard_map/all_gather | solution.py:42
  130.3 57.7 %all-gather.9.cloned.1.call-done = bf16[1024,1408]{1,0:T(8,128)(2,1)} async-done(((bf16[128,1408]{1,0:T(8,128)(2,1)}), bf16[1024,1408]{1,0:T(8,128)(2,1)}) %all-gather.9.cloned.1.call-update) | async-done | bytes 2883600 | tf_op jit(solution)/shard_map/all_gather | solution.py:12
  188.0 5.4 %convolution_convert_fusion.1 = bf16[256,1024]{1,0:T(8,128)(2,1)} fusion(bf16[1408,1024]{1,0:T(8,128)(2,1)} %all-gather.11.cloned.1.call-done, bf16[256,1024]{1,0:T(8,128)(2,1)S(1)} %all_gather.24, bf16[1024,1408]{1,0:T(8,128)(2,1)} %all-gather.9.cloned.1.call-done, f32[256,1408]{1,0:T(8,128)S(1)} %fusion.20), kind=kOutput, calls=%fused_computation.7 | convolution fusion | flops 1478819840 | bytes 8257536 | tf_op jit(solution)/shard_map/dot_general | solution.py:68
  193.3 0.0 copy-start.2
  193.4 0.0 reduce-scatter.3.cloned.1.call-update
  193.4 0.0 all-gather.13.cloned.1.call-start
  193.4 0.5 all-gather.13.cloned.1.call-update
  194.0 0.0 all-gather.15.cloned.1.call-start
  194.0 0.5 all-gather.15.cloned.1.call-update
  194.5 0.0 all-gather.17.cloned.1.call-start
  194.6 0.7 all-gather.17.cloned.1.call-update
  195.3 0.0 reduce-scatter.5.cloned.1.call-start
  195.3 5.0 %reduce-scatter.3.cloned.1.call-done = bf16[128,1024]{1,0:T(8,128)(2,1)} async-done(((bf16[256,1024]{1,0:T(8,128)(2,1)}), bf16[128,1024]{1,0:T(8,128)(2,1)}) %reduce-scatter.3.cloned.1.call-update) | async-done | bytes 262160 | tf_op jit(solution)/shard_map/reduce_scatter | solution.py:70
  200.4 0.0 copy-done
  200.4 0.0 copy-done.1
  200.4 1.1 add_convert_fusion.1
  201.5 2.2 all_gather.28
  203.7 0.2 fusion.2
  203.9 56.8 %all-gather.13.cloned.1.call-done = bf16[1024,1408]{1,0:T(8,128)(2,1)} async-done(((bf16[128,1408]{1,0:T(8,128)(2,1)}), bf16[1024,1408]{1,0:T(8,128)(2,1)}) %all-gather.13.cloned.1.call-update) | async-done | bytes 2883600 | tf_op jit(solution)/shard_map/all_gather | solution.py:12
  260.6 0.0 copy-done.2
  260.6 2.9 fusion.16
  263.5 0.0 copy-start.3
  263.5 55.2 %all-gather.15.cloned.1.call-done = bf16[1024,1408]{1,0:T(8,128)(2,1)} async-done(((bf16[128,1408]{1,0:T(8,128)(2,1)}), bf16[1024,1408]{1,0:T(8,128)(2,1)}) %all-gather.15.cloned.1.call-update) | async-done | bytes 2883600 | tf_op jit(solution)/shard_map/all_gather | solution.py:12
  318.7 60.9 %all-gather.17.cloned.1.call-done = bf16[1408,1024]{1,0:T(8,128)(2,1)} async-done(((bf16[1408,128]{1,0:T(8,128)(2,1)}), bf16[1408,1024]{1,0:T(8,128)(2,1)}) %all-gather.17.cloned.1.call-update) | async-done | bytes 2883600 | tf_op jit(solution)/shard_map/all_gather | solution.py:42
  379.6 5.4 %convolution_convert_fusion = bf16[256,1024]{1,0:T(8,128)(2,1)} fusion(bf16[1408,1024]{1,0:T(8,128)(2,1)} %all-gather.17.cloned.1.call-done, bf16[1024,1408]{1,0:T(8,128)(2,1)} %all-gather.15.cloned.1.call-done, f32[256,1408]{1,0:T(8,128)S(1)} %fusion.16, bf16[256,1024]{1,0:T(8,128)(2,1)S(1)} %all_gather.28, f32[1024]{0:T(1024)S(1)} %copy-done.2, ...), kind=kOutput, calls=%fused_computation.6 | convolution fusion | flops 1479868416 | bytes 8262656 | tf_op jit(solution)/shard_map/dot_general | solution.py:80
  385.0 0.0 reduce-scatter.5.cloned.1.call-update
  385.1 6.5 %reduce-scatter.5.cloned.1.call-done = bf16[256,512]{1,0:T(8,128)(2,1)} async-done(((bf16[256,1024]{1,0:T(8,128)(2,1)}), bf16[256,512]{1,0:T(8,128)(2,1)}) %reduce-scatter.5.cloned.1.call-update) | async-done | bytes 262160 | tf_op jit(solution)/shard_map/reduce_scatter | solution.py:81
  391.5 1.1 fusion.7
  392.7 2.5 psum.7
  395.1 0.0 copy-done.3
  395.1 1.8 fusion.9
  (3 shorter events, 0.0 us)
Async XLA Ops:
  6.5 62.8 %all-gather.7.cloned.1.call-start = ((), (), s32[]{:S(2)}) async-start(), calls=%async_computation.2 | async-start | bytes 3244032 | tf_op jit(solution)/shard_map/all_gather | solution.py:12
  7.3 123.0 %all-gather.11.cloned.1.call-start = ((), (), s32[]{:S(2)}) async-start(), calls=%async_computation.4 | async-start | bytes 3244032 | tf_op jit(solution)/shard_map/all_gather | solution.py:42
  8.0 179.9 %all-gather.9.cloned.1.call-start = ((), (), s32[]{:S(2)}) async-start(), calls=%async_computation.3 | async-start | bytes 3244032 | tf_op jit(solution)/shard_map/all_gather | solution.py:12
  8.7 191.7 %reduce-scatter.3.cloned.1.call-start = ((), (), s32[]{:S(2)}) async-start(), calls=%async_computation.5 | async-start | bytes 786432 | tf_op jit(solution)/shard_map/reduce_scatter | solution.py:70
  72.2 128.2 %copy-start = (bf16[128,1024]{1,0:T(8,128)(2,1)S(1)}, bf16[128,1024]{1,0:T(8,128)(2,1)}, u32[]{:S(2)}) copy-start(bf16[128,1024]{1,0:T(8,128)(2,1)} %param.11) | copy-start | bytes 786436
  72.2 128.2 %copy-start.1 = (bf16[256,1024]{1,0:T(8,128)(2,1)S(1)}, bf16[256,1024]{1,0:T(8,128)(2,1)}, u32[]{:S(2)}) copy-start(bf16[256,1024]{1,0:T(8,128)(2,1)} %param.12) | copy-start | bytes 1572868
  193.3 67.3 %copy-start.2 = (f32[1024]{0:T(1024)S(1)}, f32[1024]{0:T(1024)}, u32[]{:S(2)}) copy-start(f32[1024]{0:T(1024)} %param.17) | copy-start | bytes 12292
  193.4 67.3 %all-gather.13.cloned.1.call-start = ((), (), s32[]{:S(2)}) async-start(), calls=%async_computation.6 | async-start | bytes 3244032 | tf_op jit(solution)/shard_map/all_gather | solution.py:12
  194.0 124.7 %all-gather.15.cloned.1.call-start = ((), (), s32[]{:S(2)}) async-start(), calls=%async_computation.7 | async-start | bytes 3244032 | tf_op jit(solution)/shard_map/all_gather | solution.py:12
  194.5 185.1 %all-gather.17.cloned.1.call-start = ((), (), s32[]{:S(2)}) async-start(), calls=%async_computation.8 | async-start | bytes 3244032 | tf_op jit(solution)/shard_map/all_gather | solution.py:42
  195.3 196.2 %reduce-scatter.5.cloned.1.call-start = ((), (), s32[]{:S(2)}) async-start(), calls=%async_computation.9 | async-start | bytes 786432 | tf_op jit(solution)/shard_map/reduce_scatter | solution.py:81
  263.5 131.6 %copy-start.3 = (f32[512]{0:T(512)S(1)}, f32[512]{0:T(512)}, u32[]{:S(2)}) copy-start(f32[512]{0:T(512)} %param.21) | copy-start | bytes 6148
Sparse Core Ops, SparseCore 0:
  9.5 59.8 all-gather.6
  71.4 58.8 all-gather.10
  132.5 55.4 all-gather.8
  193.5 6.8 reduce-scatter.2
  202.4 58.1 all-gather.12
  262.7 55.9 all-gather.14
  320.8 58.8 all-gather.16
  385.2 6.3 reduce-scatter.4
where the time goes:
time: 404 us
  waiting for transfers between devices  360 us (89%)
  matrix products  16.5 us (4%)
  between operations  13.6 us (3%)
  blocking collectives  6.98 us (2%)
  other arithmetic  6.36 us (2%)
    all_gather x4, waiting for transfers between devices, gathered(): return lax.all_gather(part, axis, axis=dim, tiled=True)  226 us
    all_gather x2, waiting for transfers between devices, outer_weight(): return lax.all_gather(w_down, 'fs', axis=1, tiled=True)  119 us
  transfers between devices with their start and end apart: 8, of which 8 were waited for; matrix products, arithmetic and copies ran while one was open for 2% of the time, Pallas kernels for 0%

commit v1 on v0

--- a/solution.py
+++ b/solution.py
@@ -1,6 +1,10 @@
+import functools
+
 import jax
 import jax.numpy as jnp
 from jax import lax
+from jax.experimental import pallas as pl
+from jax.experimental.pallas import tpu as pltpu
 from jax.sharding import PartitionSpec as P
 
 EPS = 1e-06
@@ -90,6 +94,325 @@
     return (floats * factor[:, None] * gain_last.astype(jnp.float32)[None, :]).astype(jnp.bfloat16)
 
 
+MESH = pl.DeviceIdType.MESH
+PLANE = 4
+LANES = 128
+
+
+def fits(mesh):
+    return mesh.shape["rep"] == 2 and mesh.shape["tp"] == 2 and mesh.shape["fs"] % 2 == 0 and mesh.shape["fs"] >= 2
+
+
+def norm_rows(floats, gain_row):
+    factor = lax.rsqrt(jnp.mean(floats * floats, axis=-1, keepdims=True) + EPS)
+    return (floats * factor * gain_row).astype(jnp.bfloat16)
+
+
+def kernel(
+    depth, width, overlap,
+    tok, mix, gain1, gain2, gain3, g1, u1, d1, g2, u2, d2,
+    out,
+    xs, mixed, normed, hid, gu, dw, outgoing, arrived, own, result, landed,
+    local_sem, y_send, up_send, down_send, wide_recv, core_send, core_recv,
+    row_send, row_recv, end_sem,
+):
+    rep, fs, tp = lax.axis_index("rep"), lax.axis_index("fs"), lax.axis_index("tp")
+    z, y = fs // 2, fs % 2
+    rows, width_all = tok.shape
+    block = g1.shape[0]
+    weights = (g1, u1, d1, g2, u2, d2)
+    partner = (rep, fs, 1 - tp)
+
+    def relative(k):
+        return ((rep + k // 2) % 2, 2 * z + (y + k % 2) % 2, tp)
+
+    up, down = (rep, fs + 2, tp), (rep, fs - 2, tp)
+
+    barrier = pltpu.get_barrier_semaphore()
+
+    def greet(device):
+        pl.semaphore_signal(barrier, inc=1, device_id=device, device_id_type=MESH)
+
+    for k in range(1, PLANE):
+        greet(relative(k))
+    greet(partner)
+
+    @pl.when(z > 0)
+    def _():
+        greet(down)
+
+    @pl.when(z < depth - 1)
+    def _():
+        greet(up)
+
+    below, above = (z + depth - 1) // depth, (2 * depth - 2 - z) // depth
+    pl.semaphore_wait(barrier, PLANE + below + above)
+
+    def quarter(which_y):
+        q = 2 * rep + which_y
+        return q * width - (q // (PLANE - 1)) * overlap
+
+    def own_part(m, which_y):
+        at = pl.ds(pl.multiple_of(quarter(which_y), LANES), width)
+        return weights[m].at[at, :] if m % 3 == 2 else weights[m].at[:, at]
+
+    def place(m, blk, half):
+        at = pl.ds(pl.multiple_of(blk * block, block), block)
+        if m % 3 == 2:
+            return dw.at[m // 3, half, :, at]
+        return gu.at[m // 3, m % 3, half, at, :]
+
+    def remote(src, dst, send, recv, device):
+        return pltpu.make_async_remote_copy(
+            src_ref=src, dst_ref=dst, send_sem=send, recv_sem=recv, device_id=device, device_id_type=MESH
+        )
+
+    def keep(m):
+        return pltpu.make_async_copy(own_part(m, y), place(m, fs, tp), local_sem.at[m])
+
+    def swap(m):
+        return remote(own_part(m, 1 - y), place(m, fs, tp), y_send.at[m], wide_recv.at[m, fs], relative(1))
+
+    def send_up(m, blk, src):
+        return remote(src, place(m, blk, tp), up_send.at[m, blk], wide_recv.at[m, blk], up)
+
+    def send_down(m, blk, src):
+        return remote(src, place(m, blk, tp), down_send.at[m, blk], wide_recv.at[m, blk], down)
+
+    def send_core(m, blk, src):
+        return remote(src, place(m, blk, tp), core_send.at[m, blk], core_recv.at[m, blk], partner)
+
+    def came(m, blk):
+        remote(place(m, blk, tp), place(m, blk, tp), core_send.at[m, blk], wide_recv.at[m, blk], partner).wait_recv()
+
+    def came_core(m, blk):
+        there = place(m, blk, 1 - tp)
+        remote(there, there, core_send.at[m, blk], core_recv.at[m, blk], partner).wait_recv()
+
+    def spread(m, blk, src, go_up=True, go_down=True):
+        if go_up:
+
+            @pl.when(z < depth - 1)
+            def _():
+                send_up(m, blk, src).start()
+
+        if go_down:
+
+            @pl.when(z > 0)
+            def _():
+                send_down(m, blk, src).start()
+
+        send_core(m, blk, src).start()
+
+    def begin(group):
+        for m in group:
+            keep(m).start()
+            spread(m, fs, own_part(m, y))
+
+    def from_side(group):
+        other = 2 * z + (1 - y)
+        for m in group:
+            came(m, other)
+            spread(m, other, place(m, other, tp))
+
+    def from_line(group, d):
+        for side in (y, 1 - y):
+            for m in group:
+
+                @pl.when(z >= d)
+                def _():
+                    blk = 2 * (z - d) + side
+                    came(m, blk)
+                    spread(m, blk, place(m, blk, tp), go_down=False)
+
+                @pl.when(z + d < depth)
+                def _():
+                    blk = 2 * (z + d) + side
+                    came(m, blk)
+                    spread(m, blk, place(m, blk, tp), go_up=False)
+
+    def ready(group):
+        for m in group:
+            keep(m).wait()
+            for blk in range(2 * depth):
+                came_core(m, blk)
+
+    def rows_to(phase, k, src, dst):
+        return remote(src, dst, row_send.at[phase, k], row_recv.at[phase, k], relative(k))
+
+    def normalize_all(first, rest, gain):
+        gain_row = gain[...]
+
+        def chunk(i, carry):
+            normed[pl.ds(i * rows, rows), :] = norm_rows(rest[i].astype(jnp.float32), gain_row)
+            return carry
+
+        normed[pl.ds(0, rows), :] = norm_rows(first.astype(jnp.float32), gain_row)
+        lax.fori_loop(1, PLANE, chunk, 0)
+
+    def multiply(layer):
+        lanes = lax.broadcasted_iota(jnp.int32, (2 * rows, width), 1)
+        counted = lanes >= overlap * ((2 * rep + y) // (PLANE - 1))
+
+        def inner(i, carry):
+            half, at = i // 2, pl.ds(pl.multiple_of((i % 2) * 2 * rows, 2 * rows), 2 * rows)
+            columns = normed[at, :]
+            gate = jnp.dot(columns, gu[layer, 0, half], preferred_element_type=jnp.float32)
+            value = jnp.dot(columns, gu[layer, 1, half], preferred_element_type=jnp.float32)
+            hidden = gate / (1.0 + jnp.exp(-gate)) * value
+            hid[half, at, :] = jnp.where(counted, hidden, 0.0).astype(jnp.bfloat16)
+            return carry
+
+        lax.fori_loop(0, 4, inner, 0)
+        for k in range(PLANE - 1, -1, -1):
+            at = pl.ds(k * rows, rows)
+            part = jnp.dot(hid[0, at, :], dw[layer, 0], preferred_element_type=jnp.float32)
+            part = part + jnp.dot(hid[1, at, :], dw[layer, 1], preferred_element_type=jnp.float32)
+            if k:
+                outgoing[layer, k] = part.astype(jnp.bfloat16)
+                rows_to(1 + 2 * layer, k, outgoing.at[layer, k], arrived.at[layer, k]).start()
+            else:
+                own[...] = part
+
+    def rows_came(phase, dst):
+        for k in range(1, PLANE):
+            rows_to(phase, k, dst.at[k], dst.at[k]).wait_recv()
+
+    def total(layer):
+        summed = own[...]
+        for k in range(1, PLANE):
+            summed = summed + arrived[layer, k].astype(jnp.float32)
+        return summed
+
+    one, two = (0, 1, 2), (3, 4, 5)
+    for m in one:
+        swap(m).start()
+    begin(one)
+    for k in (3, 2, 1):
+        rows_to(0, k, tok, xs.at[k]).start()
+    for m in two:
+        swap(m).start()
+    from_side(one)
+    for d in range(1, depth):
+        from_line(one, d)
+    begin(two)
+    from_side(two)
+    rows_came(0, xs)
+    normalize_all(tok[...], xs, gain1)
+    ready(one)
+    multiply(0)
+    if depth > 1:
+        from_line(two, 1)
+    rows_came(1, arrived.at[0])
+    after_one = (tok[...].astype(jnp.float32) + 0.5 * total(0)).astype(jnp.bfloat16)
+    own_mix = mix[pl.ds(pl.multiple_of(tp * rows, rows), rows), :]
+    mixed[0] = (after_one.astype(jnp.float32) + own_mix.astype(jnp.float32)).astype(jnp.bfloat16)
+    for k in (3, 2, 1):
+        rows_to(2, k, mixed.at[0], mixed.at[k]).start()
+    for d in range(2, depth):
+        from_line(two, d)
+    rows_came(2, mixed)
+    normalize_all(mixed[0], mixed, gain2)
+    ready(two)
+    multiply(1)
+    rows_came(3, arrived.at[1])
+    after_two = (mixed[0].astype(jnp.float32) + 0.5 * total(1)).astype(jnp.bfloat16)
+    final = norm_rows(after_two.astype(jnp.float32), gain3[...])
+    share = width_all // 2
+    result[0] = final[:, :share]
+    result[1] = final[:, share:]
+    over = remote(result.at[1 - tp], landed, end_sem.at[0], end_sem.at[1], partner)
+    over.start()
+    out[pl.ds(pl.multiple_of(tp * rows, rows), rows), :] = result[tp]
+
+    for m in range(6):
+        swap(m).wait_send()
+        for blk in range(2 * depth):
+            send_core(m, blk, place(m, blk, tp)).wait_send()
+
+            @pl.when((z < depth - 1) & (blk // 2 <= z))
+            def _():
+                send_up(m, blk, place(m, blk, tp)).wait_send()
+
+            @pl.when((z > 0) & (blk // 2 >= z))
+            def _():
+                send_down(m, blk, place(m, blk, tp)).wait_send()
+
+    for phase, src in enumerate((xs, outgoing.at[0], mixed, outgoing.at[1])):
+        for k in range(1, PLANE):
+            rows_to(phase, k, src.at[k], src.at[k]).wait_send()
+    over.wait_send()
+    over.wait_recv()
+    out[pl.ds(pl.multiple_of((1 - tp) * rows, rows), rows), :] = landed[...]
+
+
+def fused(
+    tokens,
+    mixer_out,
+    gain_first,
+    gate_first,
+    up_first,
+    down_first,
+    gain_second,
+    gate_second,
+    up_second,
+    down_second,
+    gain_last,
+):
+    rows, features = tokens.shape
+    block, hidden = gate_first.shape
+    blocks = lax.axis_size("fs")
+    width = -(-hidden // (PLANE * LANES)) * LANES
+    last = lax.all_gather(gain_last, "tp", axis=0, tiled=True)
+    vmem, anywhere = pl.BlockSpec(memory_space=pltpu.VMEM), pl.BlockSpec(memory_space=pl.ANY)
+    half = jnp.bfloat16
+    sems = pltpu.SemaphoreType.DMA
+    return pl.pallas_call(
+        functools.partial(kernel, blocks // 2, width, PLANE * width - hidden),
+        out_shape=jax.ShapeDtypeStruct((2 * rows, features // 2), half),
+        in_specs=[vmem] * 5 + [anywhere] * 6,
+        out_specs=vmem,
+        scratch_shapes=[
+            pltpu.VMEM((PLANE, rows, features), half),
+            pltpu.VMEM((PLANE, rows, features), half),
+            pltpu.VMEM((PLANE * rows, features), half),
+            pltpu.VMEM((2, PLANE * rows, width), half),
+            pltpu.VMEM((2, 2, 2, features, width), half),
+            pltpu.VMEM((2, 2, width, features), half),
+            pltpu.VMEM((2, PLANE, rows, features), half),
+            pltpu.VMEM((2, PLANE, rows, features), half),
+            pltpu.VMEM((rows, features), jnp.float32),
+            pltpu.VMEM((2, rows, features // 2), half),
+            pltpu.VMEM((rows, features // 2), half),
+            sems((6,)),
+            sems((6,)),
+            sems((6, blocks)),
+            sems((6, blocks)),
+            sems((6, blocks)),
+            sems((6, blocks)),
+            sems((6, blocks)),
+            sems((4, PLANE)),
+            sems((4, PLANE)),
+            sems((2,)),
+        ],
+        compiler_params=pltpu.CompilerParams(
+            collective_id=0, has_side_effects=True, vmem_limit_bytes=48 * 1024 * 1024
+        ),
+    )(
+        tokens,
+        mixer_out,
+        gain_first[None, :],
+        gain_second[None, :],
+        last[None, :],
+        gate_first,
+        up_first,
+        down_first,
+        gate_second,
+        up_second,
+        down_second,
+    )
+
+
 def solution(mesh):
     in_specs = (
         P(("rep", "fs", "tp"), None),
@@ -105,4 +428,5 @@
         P("tp"),
     )
     out_specs = P(("rep", "fs"), "tp")
-    return jax.shard_map(local, mesh=mesh, in_specs=in_specs, out_specs=out_specs, check_vma=False)
+    body = fused if fits(mesh) else local
+    return jax.shard_map(body, mesh=mesh, in_specs=in_specs, out_specs=out_specs, check_vma=False)

time: 404 us -> 119 us (0.29)
  waiting for transfers between devices: 360 us -> 0 us
  Pallas kernels: 0 us -> 107 us
  matrix products: 16.5 us -> 0 us
  between operations: 13.6 us -> 0.02 us
  local copies, waits for them, and re-layouts: 0.02 us -> 9.29 us
  other arithmetic: 6.36 us -> 0 us
  blocking collectives: 6.98 us -> 2.1 us
    all_gather x6 -> x0, waiting for transfers between devices: 345 us -> none  [the longest x4 226 us: gathered(): return lax.all_gather(part, axis, axis=dim, tiled=True)]
    pallas_call x0 -> x1, Pallas kernels: none -> 107 us  [fused(): pl.pallas_call(functools.partial(kernel, blocks // 2, width, PLANE * widt...]
    dot_general x4 -> x0, matrix products: 16.5 us -> none  [the longest x2 5.65 us: add_both(): jnp.dot(columns, pieces[0], preferred_element_type=jnp.float32)]
    reduce_scatter x2 -> x0, waiting for transfers between devices: 11.5 us -> none  [the longest x1 6.48 us: local(): lax.psum_scatter(terms_two.astype(jnp.bfloat16), 'tp', scatter_dimension=...]
    unnamed x8 -> x23, local copies, waits for them, and re-layouts: 0.02 us -> 9.29 us
  transfers between devices with their start and end apart: 8 -> 0, of which waited for: 8 -> 0; matrix products, arithmetic and copies ran while one was open for 2% -> 0% of each run, Pallas kernels for 0% -> 0%
where the time goes in v1:
time: 119 us; the launch traced here: 118 us
  Pallas kernels  107 us (90%)
  local copies, waits for them, and re-layouts  9.29 us (8%)
  blocking collectives  2.1 us (2%)
    pallas_call x1, Pallas kernels, fused(): pl.pallas_call(functools.partial(kernel, blocks // 2, width, PLANE * widt...  107 us
    unnamed x23, local copies, waits for them, and re-layouts  9.29 us

profile of v1, /device:TPU:0, one launch (start us, length us, event | category | flops | bytes accessed | tf_op | source)
XLA Modules:
  0.0 118.4 jit_solution(16610275268122238598)
XLA Ops:
  0.0 0.0 copy-start.10
  0.0 0.0 copy-start.9
  0.0 0.7 copy-done.10
  0.7 0.0 copy-start.8
  0.7 2.1 %all-gather = f32[2,1,512]{2,1,0:T(1,128)S(1)} all-gather(f32[1,1,512]{2,1,0:T(1,128)S(1)} %bitcast.7), channel_id=1, replica_groups=mesh['rep'=2,'fs'=8,'tp'=2] {'tp'}, dimensions={0}, use_global_device_ids=true | all-gather | bytes 6144 | tf_op jit(solution)/shard_map/all_gather | solution.py:366
  2.8 0.0 copy-done.9
  2.8 0.0 copy-done.8
  2.8 0.0 copy-start
  2.8 1.0 copy-done
  3.8 0.0 copy-start.1
  3.8 1.0 copy-done.1
  4.8 0.0 copy-start.2
  4.8 1.0 copy-done.2
  5.8 0.0 copy-start.3
  5.8 1.0 copy-done.3
  6.8 0.0 copy-start.4
  6.8 1.0 copy-done.4
  7.8 0.0 copy-start.5
  7.8 1.0 copy-done.5
  8.8 0.0 copy-start.6
  8.8 1.0 copy-done.6
  9.7 0.0 copy-start.7
  9.7 0.9 copy-done.7
  10.7 106.9 %shard_map.109 = bf16[256,512]{1,0:T(8,128)(2,1)S(1)} custom-call(bf16[128,1024]{1,0:T(8,128)(2,1)S(1)} %copy-done.7, bf16[256,1024]{1,0:T(8,128)(2,1)S(1)} %copy-done, f32[1,1024]{1,0:T(1,128)S(1)} %bitcast.5, f32[1,1024]{1,0:T(1,128)S(1)} %bitcast.6, f32[1,1024]{1,0:T(1,128)S(1)} %bitcast.4, bf16[128,1408]{1,0:T(8,128)(2,1)S(1)} %copy-done.1, ...), custom_call_target="tpu_custom_call" | custom-call | tf_op jit(solution)/shard_map/pallas_call | solution.py:370
  117.6 0.7 copy.13
Async XLA Ops:
  0.0 0.7 copy-start.10
  0.0 2.8 %copy-start.9 = (f32[1024]{0:T(1024)S(1)}, f32[1024]{0:T(1024)}, u32[]{:S(2)}) copy-start(f32[1024]{0:T(1024)} %param.17) | copy-start | bytes 12292
  0.7 2.1 %copy-start.8 = (f32[1024]{0:T(1024)S(1)}, f32[1024]{0:T(1024)}, u32[]{:S(2)}) copy-start(f32[1024]{0:T(1024)} %param.13) | copy-start | bytes 12292
  2.8 1.0 copy-start
  3.8 1.0 copy-start.1
  4.8 1.0 copy-start.2
  5.8 1.0 copy-start.3
  6.8 1.0 copy-start.4
  7.8 1.0 copy-start.5
  8.8 1.0 copy-start.6
  9.7 0.9 copy-start.7

commit v2 on v1

--- a/solution.py
+++ b/solution.py
@@ -110,15 +110,15 @@
 
 def kernel(
     depth, width, overlap,
-    tok, mix, gain1, gain2, gain3, g1, u1, d1, g2, u2, d2,
+    tokens, mixer, gains1, gains2, gains3, g1, u1, d1, g2, u2, d2,
     out,
-    xs, mixed, normed, hid, gu, dw, outgoing, arrived, own, result, landed,
+    mix, gain1, gain2, gain3, xs, mixed, normed, hid, gu, dw, outgoing, arrived, own, result, landed,
     local_sem, y_send, up_send, down_send, wide_recv, core_send, core_recv,
-    row_send, row_recv, end_sem,
+    row_send, row_recv, part_send, part_recv, end_sem,
 ):
     rep, fs, tp = lax.axis_index("rep"), lax.axis_index("fs"), lax.axis_index("tp")
     z, y = fs // 2, fs % 2
-    rows, width_all = tok.shape
+    rows, width_all = tokens.shape
     block = g1.shape[0]
     weights = (g1, u1, d1, g2, u2, d2)
     partner = (rep, fs, 1 - tp)
@@ -127,6 +127,22 @@
         return ((rep + k // 2) % 2, 2 * z + (y + k % 2) % 2, tp)
 
     up, down = (rep, fs + 2, tp), (rep, fs - 2, tp)
+
+    own_rows = pl.ds(pl.multiple_of(tp * rows, rows), rows)
+    loads = [
+        pltpu.make_async_copy(src, dst, local_sem.at[6 + i])
+        for i, (src, dst) in enumerate(
+            (
+                (tokens, xs.at[0]),
+                (mixer.at[own_rows, :], mix),
+                (gains1, gain1),
+                (gains2, gain2),
+                (gains3, gain3.at[tp]),
+            )
+        )
+    ]
+    for load in loads:
+        load.start()
 
     barrier = pltpu.get_barrier_semaphore()
 
@@ -240,21 +256,20 @@
     def rows_to(phase, k, src, dst):
         return remote(src, dst, row_send.at[phase, k], row_recv.at[phase, k], relative(k))
 
-    def normalize_all(first, rest, gain):
+    def normalize_all(source, gain):
         gain_row = gain[...]
 
         def chunk(i, carry):
-            normed[pl.ds(i * rows, rows), :] = norm_rows(rest[i].astype(jnp.float32), gain_row)
+            normed[pl.ds(pl.multiple_of(i * rows, rows), rows), :] = norm_rows(source[i].astype(jnp.float32), gain_row)
             return carry
 
-        normed[pl.ds(0, rows), :] = norm_rows(first.astype(jnp.float32), gain_row)
-        lax.fori_loop(1, PLANE, chunk, 0)
-
-    def multiply(layer):
+        lax.fori_loop(0, PLANE, chunk, 0)
+
+    def inner(layer):
         lanes = lax.broadcasted_iota(jnp.int32, (2 * rows, width), 1)
         counted = lanes >= overlap * ((2 * rep + y) // (PLANE - 1))
 
-        def inner(i, carry):
+        def piece(i, carry):
             half, at = i // 2, pl.ds(pl.multiple_of((i % 2) * 2 * rows, 2 * rows), 2 * rows)
             columns = normed[at, :]
             gate = jnp.dot(columns, gu[layer, 0, half], preferred_element_type=jnp.float32)
@@ -263,67 +278,116 @@
             hid[half, at, :] = jnp.where(counted, hidden, 0.0).astype(jnp.bfloat16)
             return carry
 
-        lax.fori_loop(0, 4, inner, 0)
+        lax.fori_loop(0, 4, piece, 0)
+
+    def share_of(layer, k, zz):
+        at = pl.ds(pl.multiple_of(zz * 2 * block, 2 * block), 2 * block)
+        return remote(
+            outgoing.at[layer, k, :, at],
+            arrived.at[layer, k, :, at],
+            part_send.at[layer, k, zz],
+            part_recv.at[layer, k, zz],
+            relative(k),
+        )
+
+    def outer(layer, zz):
+        for which in range(2):
+            came_core(3 * layer + 2, 2 * zz + which)
+        at = pl.ds(pl.multiple_of(zz * 2 * block, 2 * block), 2 * block)
+        part = jnp.dot(hid[0], dw[layer, 0, :, at], preferred_element_type=jnp.float32)
+        part = part + jnp.dot(hid[1], dw[layer, 1, :, at], preferred_element_type=jnp.float32)
         for k in range(PLANE - 1, -1, -1):
-            at = pl.ds(k * rows, rows)
-            part = jnp.dot(hid[0, at, :], dw[layer, 0], preferred_element_type=jnp.float32)
-            part = part + jnp.dot(hid[1, at, :], dw[layer, 1], preferred_element_type=jnp.float32)
+            mine = part[k * rows : (k + 1) * rows]
             if k:
-                outgoing[layer, k] = part.astype(jnp.bfloat16)
-                rows_to(1 + 2 * layer, k, outgoing.at[layer, k], arrived.at[layer, k]).start()
+                outgoing[layer, k, :, at] = mine.astype(jnp.bfloat16)
+                share_of(layer, k, zz).start()
             else:
-                own[...] = part
+                own[:, at] = mine
+
+    def outer_at(layer, d):
+        if d == 0:
+            keep(3 * layer + 2).wait()
+            outer(layer, z)
+            return
+
+        @pl.when(z >= d)
+        def _():
+            outer(layer, z - d)
+
+        @pl.when(z + d < depth)
+        def _():
+            outer(layer, z + d)
 
     def rows_came(phase, dst):
         for k in range(1, PLANE):
             rows_to(phase, k, dst.at[k], dst.at[k]).wait_recv()
 
     def total(layer):
+        for k in range(1, PLANE):
+            for zz in range(depth):
+                share_of(layer, k, zz).wait_recv()
         summed = own[...]
         for k in range(1, PLANE):
             summed = summed + arrived[layer, k].astype(jnp.float32)
         return summed
 
     one, two = (0, 1, 2), (3, 4, 5)
+    swap_gain = remote(gains3, gain3.at[tp], end_sem.at[2], end_sem.at[3], partner)
     for m in one:
         swap(m).start()
     begin(one)
     for k in (3, 2, 1):
-        rows_to(0, k, tok, xs.at[k]).start()
+        rows_to(0, k, tokens, xs.at[k]).start()
     for m in two:
         swap(m).start()
+    swap_gain.start()
     from_side(one)
     for d in range(1, depth):
         from_line(one, d)
     begin(two)
     from_side(two)
+    for load in loads:
+        load.wait()
     rows_came(0, xs)
-    normalize_all(tok[...], xs, gain1)
-    ready(one)
-    multiply(0)
+    normalize_all(xs, gain1)
+    ready(one[:2])
+    inner(0)
+    for d in range(depth):
+        outer_at(0, d)
     if depth > 1:
-        from_line(two, 1)
-    rows_came(1, arrived.at[0])
-    after_one = (tok[...].astype(jnp.float32) + 0.5 * total(0)).astype(jnp.bfloat16)
-    own_mix = mix[pl.ds(pl.multiple_of(tp * rows, rows), rows), :]
-    mixed[0] = (after_one.astype(jnp.float32) + own_mix.astype(jnp.float32)).astype(jnp.bfloat16)
+        from_line(two[:2], 1)
+    after_one = (xs[0].astype(jnp.float32) + 0.5 * total(0)).astype(jnp.bfloat16)
+    mixed[0] = (after_one.astype(jnp.float32) + mix[...].astype(jnp.float32)).astype(jnp.bfloat16)
     for k in (3, 2, 1):
-        rows_to(2, k, mixed.at[0], mixed.at[k]).start()
-    for d in range(2, depth):
-        from_line(two, d)
-    rows_came(2, mixed)
-    normalize_all(mixed[0], mixed, gain2)
-    ready(two)
-    multiply(1)
-    rows_came(3, arrived.at[1])
+        rows_to(1, k, mixed.at[0], mixed.at[k]).start()
+    for d in range(2, depth - 1):
+        from_line(two[:2], d)
+    if depth > 2:
+        from_line(two[2:], 1)
+    rows_came(1, mixed)
+    normalize_all(mixed, gain2)
+    if depth > 2:
+        from_line(two[:2], depth - 1)
+    elif depth > 1:
+        from_line(two[2:], 1)
+    ready(two[:2])
+    inner(1)
+    outer_at(1, 0)
+    for d in range(1, depth):
+        if d > 1:
+            from_line(two[2:], d)
+        outer_at(1, d)
     after_two = (mixed[0].astype(jnp.float32) + 0.5 * total(1)).astype(jnp.bfloat16)
-    final = norm_rows(after_two.astype(jnp.float32), gain3[...])
+    floats = after_two.astype(jnp.float32)
+    floats = floats * lax.rsqrt(jnp.mean(floats * floats, axis=-1, keepdims=True) + EPS)
     share = width_all // 2
-    result[0] = final[:, :share]
-    result[1] = final[:, share:]
+    swap_gain.wait_send()
+    remote(gain3.at[1 - tp], gain3.at[1 - tp], end_sem.at[2], end_sem.at[3], partner).wait_recv()
+    result[0] = (floats[:, :share] * gain3[0]).astype(jnp.bfloat16)
+    result[1] = (floats[:, share:] * gain3[1]).astype(jnp.bfloat16)
     over = remote(result.at[1 - tp], landed, end_sem.at[0], end_sem.at[1], partner)
     over.start()
-    out[pl.ds(pl.multiple_of(tp * rows, rows), rows), :] = result[tp]
+    out[own_rows, :] = result[tp]
 
     for m in range(6):
         swap(m).wait_send()
@@ -338,9 +402,11 @@
             def _():
                 send_down(m, blk, place(m, blk, tp)).wait_send()
 
-    for phase, src in enumerate((xs, outgoing.at[0], mixed, outgoing.at[1])):
+    for phase, src in enumerate((xs, mixed)):
         for k in range(1, PLANE):
             rows_to(phase, k, src.at[k], src.at[k]).wait_send()
+            for zz in range(depth):
+                share_of(phase, k, zz).wait_send()
     over.wait_send()
     over.wait_recv()
     out[pl.ds(pl.multiple_of((1 - tp) * rows, rows), rows), :] = landed[...]
@@ -363,16 +429,19 @@
     block, hidden = gate_first.shape
     blocks = lax.axis_size("fs")
     width = -(-hidden // (PLANE * LANES)) * LANES
-    last = lax.all_gather(gain_last, "tp", axis=0, tiled=True)
-    vmem, anywhere = pl.BlockSpec(memory_space=pltpu.VMEM), pl.BlockSpec(memory_space=pl.ANY)
+    vmem, anywhere = pl.BlockSpec(memory_space=pltpu.VMEM), pl.BlockSpec(memory_space=pltpu.HBM)
     half = jnp.bfloat16
     sems = pltpu.SemaphoreType.DMA
     return pl.pallas_call(
         functools.partial(kernel, blocks // 2, width, PLANE * width - hidden),
         out_shape=jax.ShapeDtypeStruct((2 * rows, features // 2), half),
-        in_specs=[vmem] * 5 + [anywhere] * 6,
+        in_specs=[anywhere] * 11,
         out_specs=vmem,
         scratch_shapes=[
+            pltpu.VMEM((rows, features), half),
+            pltpu.VMEM((1, features), jnp.float32),
+            pltpu.VMEM((1, features), jnp.float32),
+            pltpu.VMEM((2, 1, features // 2), jnp.float32),
             pltpu.VMEM((PLANE, rows, features), half),
             pltpu.VMEM((PLANE, rows, features), half),
             pltpu.VMEM((PLANE * rows, features), half),
@@ -384,26 +453,28 @@
             pltpu.VMEM((rows, features), jnp.float32),
             pltpu.VMEM((2, rows, features // 2), half),
             pltpu.VMEM((rows, features // 2), half),
-            sems((6,)),
+            sems((11,)),
             sems((6,)),
             sems((6, blocks)),
             sems((6, blocks)),
             sems((6, blocks)),
             sems((6, blocks)),
             sems((6, blocks)),
-            sems((4, PLANE)),
-            sems((4, PLANE)),
-            sems((2,)),
+            sems((2, PLANE)),
+            sems((2, PLANE)),
+            sems((2, PLANE, blocks // 2)),
+            sems((2, PLANE, blocks // 2)),
+            sems((4,)),
         ],
         compiler_params=pltpu.CompilerParams(
-            collective_id=0, has_side_effects=True, vmem_limit_bytes=48 * 1024 * 1024
+            collective_id=0, has_side_effects=True, vmem_limit_bytes=67_043_328
         ),
     )(
         tokens,
         mixer_out,
         gain_first[None, :],
         gain_second[None, :],
-        last[None, :],
+        gain_last[None, :],
         gate_first,
         up_first,
         down_first,

time: 119 us -> 101 us (0.85)
  local copies, waits for them, and re-layouts: 9.29 us -> 1.67 us
  Pallas kernels: 107 us -> 99.5 us
  blocking collectives: 2.1 us -> 0 us
    unnamed x23 -> x1, local copies, waits for them, and re-layouts: 9.29 us -> 1.67 us
    pallas_call x1, Pallas kernels: 107 us -> 99.5 us  [fused(): pl.pallas_call(functools.partial(kernel, blocks // 2, width, PLANE * widt...]
    all_gather x1 -> x0, blocking collectives: 2.1 us -> none  [fused(): last = lax.all_gather(gain_last, 'tp', axis=0, tiled=True)]
where the time goes in v2:
time: 101 us
  Pallas kernels  99.5 us (99%)
  local copies, waits for them, and re-layouts  1.67 us (2%)
    pallas_call x1, Pallas kernels, fused(): pl.pallas_call(functools.partial(kernel, blocks // 2, width, PLANE * widt...  99.5 us

profile of v2, /device:TPU:0, one launch (start us, length us, event | category | flops | bytes accessed | tf_op | source)
XLA Modules:
  0.0 101.2 jit_solution(15514312768623569535)
XLA Ops:
  0.0 99.5 %shard_map.109 = bf16[256,512]{1,0:T(8,128)(2,1)} custom-call(bf16[128,1024]{1,0:T(8,128)(2,1)} %tokens.1, bf16[256,1024]{1,0:T(8,128)(2,1)} %mixer.1, f32[1,1024]{1,0:T(1,128)} %bitcast.3, f32[1,1024]{1,0:T(1,128)} %bitcast.4, f32[1,512]{1,0:T(1,128)} %bitcast.5, bf16[128,1408]{1,0:T(8,128)(2,1)} %g1.1, bf16[128,1408]{1,0:T(8,128)(2,1)} %u1_.1, ...), custom_call_target="tpu_custom_call" | custom-call | tf_op jit(solution)/shard_map/pallas_call | solution.py:435
  99.5 1.7 %copy.13 = bf16[256,512]{1,0:T(8,128)(2,1)} copy(bf16[256,512]{1,0:T(8,128)(2,1)} %shard_map.109) | data formatting | bytes 524288

commit v3 on v2

--- a/solution.py
+++ b/solution.py
@@ -96,11 +96,13 @@
 
 MESH = pl.DeviceIdType.MESH
 PLANE = 4
+SUBLANES = 16
 LANES = 128
+CROSS = (((1,), (1,)), ((), ()))
 
 
 def fits(mesh):
-    return mesh.shape["rep"] == 2 and mesh.shape["tp"] == 2 and mesh.shape["fs"] % 2 == 0 and mesh.shape["fs"] >= 2
+    return mesh.shape["rep"] == 2 and mesh.shape["tp"] == 2 and mesh.shape["fs"] % 2 == 0
 
 
 def norm_rows(floats, gain_row):
@@ -109,10 +111,10 @@
 
 
 def kernel(
-    depth, width, overlap,
+    depth, width,
     tokens, mixer, gains1, gains2, gains3, g1, u1, d1, g2, u2, d2,
     out,
-    mix, gain1, gain2, gain3, xs, mixed, normed, hid, gu, dw, outgoing, arrived, own, result, landed,
+    raw, turned, mix, gain1, gain2, gain3, xs, mixed, normed, hid, gu, dw, outgoing, arrived, own, result, landed,
     local_sem, y_send, up_send, down_send, wide_recv, core_send, core_recv,
     row_send, row_recv, part_send, part_recv, end_sem,
 ):
@@ -141,8 +143,18 @@
             )
         )
     ]
+    tall = (0, 1, 3, 4)
+    fetch = {m: pltpu.make_async_copy(weights[m], raw.at[i], local_sem.at[11 + i]) for i, m in enumerate(tall)}
+    for m in tall:
+        fetch[m].start()
     for load in loads:
         load.start()
+
+    def turn(group):
+        for m in group:
+            i = tall.index(m)
+            fetch[m].wait()
+            turned[i] = raw[i].T
 
     barrier = pltpu.get_barrier_semaphore()
 
@@ -164,19 +176,14 @@
     below, above = (z + depth - 1) // depth, (2 * depth - 2 - z) // depth
     pl.semaphore_wait(barrier, PLANE + below + above)
 
-    def quarter(which_y):
-        q = 2 * rep + which_y
-        return q * width - (q // (PLANE - 1)) * overlap
-
     def own_part(m, which_y):
-        at = pl.ds(pl.multiple_of(quarter(which_y), LANES), width)
-        return weights[m].at[at, :] if m % 3 == 2 else weights[m].at[:, at]
+        at = pl.ds(pl.multiple_of((2 * rep + which_y) * width, SUBLANES), width)
+        return weights[m].at[at, :] if m % 3 == 2 else turned.at[tall.index(m), at, :]
 
     def place(m, blk, half):
         at = pl.ds(pl.multiple_of(blk * block, block), block)
-        if m % 3 == 2:
-            return dw.at[m // 3, half, :, at]
-        return gu.at[m // 3, m % 3, half, at, :]
+        held = dw.at[m // 3, half] if m % 3 == 2 else gu.at[m // 3, m % 3, half]
+        return held.at[:, at]
 
     def remote(src, dst, send, recv, device):
         return pltpu.make_async_remote_copy(
@@ -266,16 +273,13 @@
         lax.fori_loop(0, PLANE, chunk, 0)
 
     def inner(layer):
-        lanes = lax.broadcasted_iota(jnp.int32, (2 * rows, width), 1)
-        counted = lanes >= overlap * ((2 * rep + y) // (PLANE - 1))
-
         def piece(i, carry):
             half, at = i // 2, pl.ds(pl.multiple_of((i % 2) * 2 * rows, 2 * rows), 2 * rows)
             columns = normed[at, :]
-            gate = jnp.dot(columns, gu[layer, 0, half], preferred_element_type=jnp.float32)
-            value = jnp.dot(columns, gu[layer, 1, half], preferred_element_type=jnp.float32)
+            gate = lax.dot_general(columns, gu[layer, 0, half], CROSS, preferred_element_type=jnp.float32)
+            value = lax.dot_general(columns, gu[layer, 1, half], CROSS, preferred_element_type=jnp.float32)
             hidden = gate / (1.0 + jnp.exp(-gate)) * value
-            hid[half, at, :] = jnp.where(counted, hidden, 0.0).astype(jnp.bfloat16)
+            hid[half, at, :] = hidden.astype(jnp.bfloat16)
             return carry
 
         lax.fori_loop(0, 4, piece, 0)
@@ -333,17 +337,21 @@
 
     one, two = (0, 1, 2), (3, 4, 5)
     swap_gain = remote(gains3, gain3.at[tp], end_sem.at[2], end_sem.at[3], partner)
-    for m in one:
+    swap(2).start()
+    begin(one[2:])
+    turn(one[:2])
+    for m in one[:2]:
         swap(m).start()
-    begin(one)
+    begin(one[:2])
     for k in (3, 2, 1):
         rows_to(0, k, tokens, xs.at[k]).start()
+    turn(two[:2])
     for m in two:
         swap(m).start()
     swap_gain.start()
-    from_side(one)
+    from_side((2, 0, 1))
     for d in range(1, depth):
-        from_line(one, d)
+        from_line((2, 0, 1), d)
     begin(two)
     from_side(two)
     for load in loads:
@@ -364,6 +372,13 @@
         from_line(two[:2], d)
     if depth > 2:
         from_line(two[2:], 1)
+    relays = (z > 0) & (z < depth - 1)
+
+    @pl.when(relays)
+    def _():
+        for d in range(2, depth):
+            from_line(two[2:], d)
+
     rows_came(1, mixed)
     normalize_all(mixed, gain2)
     if depth > 2:
@@ -375,7 +390,11 @@
     outer_at(1, 0)
     for d in range(1, depth):
         if d > 1:
-            from_line(two[2:], d)
+
+            @pl.when((z == 0) | (z == depth - 1))
+            def _():
+                from_line(two[2:], d)
+
         outer_at(1, d)
     after_two = (mixed[0].astype(jnp.float32) + 0.5 * total(1)).astype(jnp.bfloat16)
     floats = after_two.astype(jnp.float32)
@@ -428,16 +447,23 @@
     rows, features = tokens.shape
     block, hidden = gate_first.shape
     blocks = lax.axis_size("fs")
-    width = -(-hidden // (PLANE * LANES)) * LANES
+    if hidden % (PLANE * SUBLANES) or block % LANES or rows % SUBLANES:
+        return local(
+            tokens, mixer_out, gain_first, gate_first, up_first, down_first,
+            gain_second, gate_second, up_second, down_second, gain_last,
+        )
+    width = hidden // PLANE
     vmem, anywhere = pl.BlockSpec(memory_space=pltpu.VMEM), pl.BlockSpec(memory_space=pltpu.HBM)
     half = jnp.bfloat16
     sems = pltpu.SemaphoreType.DMA
     return pl.pallas_call(
-        functools.partial(kernel, blocks // 2, width, PLANE * width - hidden),
+        functools.partial(kernel, blocks // 2, width),
         out_shape=jax.ShapeDtypeStruct((2 * rows, features // 2), half),
         in_specs=[anywhere] * 11,
         out_specs=vmem,
         scratch_shapes=[
+            pltpu.VMEM((4, block, hidden), half),
+            pltpu.VMEM((4, hidden, block), half),
             pltpu.VMEM((rows, features), half),
             pltpu.VMEM((1, features), jnp.float32),
             pltpu.VMEM((1, features), jnp.float32),
@@ -446,14 +472,14 @@
             pltpu.VMEM((PLANE, rows, features), half),
             pltpu.VMEM((PLANE * rows, features), half),
             pltpu.VMEM((2, PLANE * rows, width), half),
-            pltpu.VMEM((2, 2, 2, features, width), half),
+            pltpu.VMEM((2, 2, 2, width, features), half),
             pltpu.VMEM((2, 2, width, features), half),
             pltpu.VMEM((2, PLANE, rows, features), half),
             pltpu.VMEM((2, PLANE, rows, features), half),
             pltpu.VMEM((rows, features), jnp.float32),
             pltpu.VMEM((2, rows, features // 2), half),
             pltpu.VMEM((rows, features // 2), half),
-            sems((11,)),
+            sems((15,)),
             sems((6,)),
             sems((6, blocks)),
             sems((6, blocks)),

time: 101 us -> 101 us (level)
  no operation moved by 1% of the time
where the time goes in v3:
time: 101 us
  Pallas kernels  99.2 us (98%)
  local copies, waits for them, and re-layouts  1.67 us (2%)
    pallas_call x1, Pallas kernels, fused(): pl.pallas_call(functools.partial(kernel, blocks // 2, width), out_shape=j...  99.2 us

profile of v3, /device:TPU:0, one launch (start us, length us, event | category | flops | bytes accessed | tf_op | source)
XLA Modules:
  0.0 100.9 jit_solution(15245719482010498672)
XLA Ops:
  0.0 99.2 %shard_map.109 = bf16[256,512]{1,0:T(8,128)(2,1)} custom-call(bf16[128,1024]{1,0:T(8,128)(2,1)} %tokens.1, bf16[256,1024]{1,0:T(8,128)(2,1)} %mixer.1, f32[1,1024]{1,0:T(1,128)} %bitcast.3, f32[1,1024]{1,0:T(1,128)} %bitcast.4, f32[1,512]{1,0:T(1,128)} %bitcast.5, bf16[128,1408]{1,0:T(8,128)(2,1)} %g1.1, bf16[128,1408]{1,0:T(8,128)(2,1)} %u1_.1, ...), custom_call_target="tpu_custom_call" | custom-call | tf_op jit(solution)/shard_map/pallas_call | solution.py:459
  99.3 1.7 %copy.13 = bf16[256,512]{1,0:T(8,128)(2,1)} copy(bf16[256,512]{1,0:T(8,128)(2,1)} %shard_map.109) | data formatting | bytes 524288

commit v4 on v3

--- a/solution.py
+++ b/solution.py
@@ -336,6 +336,8 @@
         return summed
 
     one, two = (0, 1, 2), (3, 4, 5)
+    relays = (z > 0) & (z < depth - 1)
+    ends = (z == 0) | (z == depth - 1)
     swap_gain = remote(gains3, gain3.at[tp], end_sem.at[2], end_sem.at[3], partner)
     swap(2).start()
     begin(one[2:])
@@ -349,9 +351,15 @@
     for m in two:
         swap(m).start()
     swap_gain.start()
-    from_side((2, 0, 1))
+    from_side(one)
     for d in range(1, depth):
-        from_line((2, 0, 1), d)
+        from_line(one[:2], d)
+
+    @pl.when(relays)
+    def _():
+        for d in range(1, depth):
+            from_line(one[2:], d)
+
     begin(two)
     from_side(two)
     for load in loads:
@@ -360,7 +368,13 @@
     normalize_all(xs, gain1)
     ready(one[:2])
     inner(0)
-    for d in range(depth):
+    outer_at(0, 0)
+    for d in range(1, depth):
+
+        @pl.when(ends)
+        def _():
+            from_line(one[2:], d)
+
         outer_at(0, d)
     if depth > 1:
         from_line(two[:2], 1)
@@ -372,8 +386,6 @@
         from_line(two[:2], d)
     if depth > 2:
         from_line(two[2:], 1)
-    relays = (z > 0) & (z < depth - 1)
-
     @pl.when(relays)
     def _():
         for d in range(2, depth):
@@ -391,7 +403,7 @@
     for d in range(1, depth):
         if d > 1:
 
-            @pl.when((z == 0) | (z == depth - 1))
+            @pl.when(ends)
             def _():
                 from_line(two[2:], d)
 

time: 101 us -> 98.3 us (0.973)
  Pallas kernels: 99.2 us -> 96.4 us
    pallas_call x1, Pallas kernels: 99.2 us -> 96.4 us  [fused(): pl.pallas_call(functools.partial(kernel, blocks // 2, width), out_shape=j...]
where the time goes in v4:
time: 98.3 us; the launch traced here: 98.1 us
  Pallas kernels  96.4 us (98%)
  local copies, waits for them, and re-layouts  1.67 us (2%)
    pallas_call x1, Pallas kernels, fused(): pl.pallas_call(functools.partial(kernel, blocks // 2, width), out_shape=j...  96.4 us

profile of v4, /device:TPU:0, one launch (start us, length us, event | category | flops | bytes accessed | tf_op | source)
XLA Modules:
  0.0 98.1 jit_solution(12748780569427562743)
XLA Ops:
  0.0 96.4 %shard_map.109 = bf16[256,512]{1,0:T(8,128)(2,1)} custom-call(bf16[128,1024]{1,0:T(8,128)(2,1)} %tokens.1, bf16[256,1024]{1,0:T(8,128)(2,1)} %mixer.1, f32[1,1024]{1,0:T(1,128)} %bitcast.3, f32[1,1024]{1,0:T(1,128)} %bitcast.4, f32[1,512]{1,0:T(1,128)} %bitcast.5, bf16[128,1408]{1,0:T(8,128)(2,1)} %g1.1, bf16[128,1408]{1,0:T(8,128)(2,1)} %u1_.1, ...), custom_call_target="tpu_custom_call" | custom-call | tf_op jit(solution)/shard_map/pallas_call | solution.py:471
  96.4 1.7 %copy.13 = bf16[256,512]{1,0:T(8,128)(2,1)} copy(bf16[256,512]{1,0:T(8,128)(2,1)} %shard_map.109) | data formatting | bytes 524288

commit v5 on v4

--- a/solution.py
+++ b/solution.py
@@ -261,7 +261,13 @@
                 came_core(m, blk)
 
     def rows_to(phase, k, src, dst):
-        return remote(src, dst, row_send.at[phase, k], row_recv.at[phase, k], relative(k))
+        return remote(src, dst, row_send.at[phase, k, 0], row_recv.at[phase, k, 0], relative(k))
+
+    def split_rows(held, there, k, h, via):
+        at = pl.ds(h * (rows // 2), rows // 2)
+        return remote(
+            mixed.at[held, at, :], mixed.at[there, at, :], row_send.at[1, k, h], row_recv.at[1, k, h], relative(via)
+        )
 
     def normalize_all(source, gain):
         gain_row = gain[...]
@@ -380,8 +386,13 @@
         from_line(two[:2], 1)
     after_one = (xs[0].astype(jnp.float32) + 0.5 * total(0)).astype(jnp.bfloat16)
     mixed[0] = (after_one.astype(jnp.float32) + mix[...].astype(jnp.float32)).astype(jnp.bfloat16)
-    for k in (3, 2, 1):
-        rows_to(1, k, mixed.at[0], mixed.at[k]).start()
+    for h in range(2):
+        split_rows(0, 2, 2, h, 2).start()
+        split_rows(0, 1, 1, 1 - h, 1).start()
+    split_rows(0, 2, 2, 0, 2).wait_recv()
+    split_rows(2, 3, 3, 0, 1).start()
+    split_rows(0, 1, 1, 1, 1).wait_recv()
+    split_rows(1, 3, 3, 1, 2).start()
     for d in range(2, depth - 1):
         from_line(two[:2], d)
     if depth > 2:
@@ -391,7 +402,10 @@
         for d in range(2, depth):
             from_line(two[2:], d)
 
-    rows_came(1, mixed)
+    split_rows(0, 2, 2, 1, 2).wait_recv()
+    split_rows(0, 1, 1, 0, 1).wait_recv()
+    split_rows(2, 3, 3, 0, 1).wait_recv()
+    split_rows(1, 3, 3, 1, 2).wait_recv()
     normalize_all(mixed, gain2)
     if depth > 2:
         from_line(two[:2], depth - 1)
@@ -433,9 +447,14 @@
             def _():
                 send_down(m, blk, place(m, blk, tp)).wait_send()
 
-    for phase, src in enumerate((xs, mixed)):
+    for h in range(2):
+        split_rows(0, 2, 2, h, 2).wait_send()
+        split_rows(0, 1, 1, h, 1).wait_send()
+        split_rows(2 - h, 3, 3, h, 1 + h).wait_send()
+    for phase in range(2):
         for k in range(1, PLANE):
-            rows_to(phase, k, src.at[k], src.at[k]).wait_send()
+            if phase == 0:
+                rows_to(phase, k, xs.at[k], xs.at[k]).wait_send()
             for zz in range(depth):
                 share_of(phase, k, zz).wait_send()
     over.wait_send()
@@ -498,8 +517,8 @@
             sems((6, blocks)),
             sems((6, blocks)),
             sems((6, blocks)),
-            sems((2, PLANE)),
-            sems((2, PLANE)),
+            sems((2, PLANE, 2)),
+            sems((2, PLANE, 2)),
             sems((2, PLANE, blocks // 2)),
             sems((2, PLANE, blocks // 2)),
             sems((4,)),

time: 98.3 us -> 98.4 us (level)
  no operation moved by 1% of the time
where the time goes in v5:
time: 98.4 us; the launch traced here: 98.3 us
  Pallas kernels  96.6 us (98%)
  local copies, waits for them, and re-layouts  1.67 us (2%)
    pallas_call x1, Pallas kernels, fused(): pl.pallas_call(functools.partial(kernel, blocks // 2, width), out_shape=j...  96.6 us

profile of v5, /device:TPU:0, one launch (start us, length us, event | category | flops | bytes accessed | tf_op | source)
XLA Modules:
  0.0 98.3 jit_solution(11184716817632534753)
XLA Ops:
  0.0 96.6 %shard_map.109 = bf16[256,512]{1,0:T(8,128)(2,1)} custom-call(bf16[128,1024]{1,0:T(8,128)(2,1)} %tokens.1, bf16[256,1024]{1,0:T(8,128)(2,1)} %mixer.1, f32[1,1024]{1,0:T(1,128)} %bitcast.3, f32[1,1024]{1,0:T(1,128)} %bitcast.4, f32[1,512]{1,0:T(1,128)} %bitcast.5, bf16[128,1408]{1,0:T(8,128)(2,1)} %g1.1, bf16[128,1408]{1,0:T(8,128)(2,1)} %u1_.1, ...), custom_call_target="tpu_custom_call" | custom-call | tf_op jit(solution)/shard_map/pallas_call | solution.py:490
  96.6 1.7 %copy.13 = bf16[256,512]{1,0:T(8,128)(2,1)} copy(bf16[256,512]{1,0:T(8,128)(2,1)} %shard_map.109) | data formatting | bytes 524288
